TPU v7x, 32 devices: a whole 2x2x4 slice. The times are simulated.
32 devices in a mesh: ep: 16 (over z, y, x), tp: 2 (over core).
Axes of the slice: x: 2, y: 2, z: 4, core: 2. Of those that a mesh axis runs over, the one named last changes fastest.
Arguments:
- tokens: bfloat16 [256, 2048], P('ep'), may hold values from -6 to 6
- state: float32 [256, 8, 128, 128], P('ep', 'tp'), may hold values from -6 to 6
- mix_gain: float32 [2048], replicated, may hold values from 0.1 to 1.9
- moe_gain: float32 [2048], replicated, may hold values from 0.1 to 1.9
- head_gain: float32 [128], replicated, may hold values from 0.1 to 1.9
- w_forget: bfloat16 [2048, 1024], P(None, 'tp'), may hold values from -0.125 to 0.125
- w_query: bfloat16 [2048, 1024], P(None, 'tp'), may hold values from -0.125 to 0.125
- w_input: bfloat16 [2048, 1024], P(None, 'tp'), may hold values from -0.125 to 0.125
- w_outgate: bfloat16 [2048, 1024], P(None, 'tp'), may hold values from -0.125 to 0.125
- lower_bound: float32 [1024], P('tp'), may hold values from 0 to 0.9
- w_mix_out: bfloat16 [1024, 2048], P('tp'), may hold values from -0.1875 to 0.1875
- routes: int32 [256, 6], P('ep'), may hold values from 0 to 15, all different within a row; in each aligned block of 16 rows (0 to 15, 16 to 31, ...) at most 16 rows name the same one
- route_scores: float32 [256, 6], P('ep'), may hold values from 0.05 to 1
- expert_gate: bfloat16 [16, 2048, 512], P('ep', None, 'tp'), may hold values from -0.125 to 0.125
- expert_up: bfloat16 [16, 2048, 512], P('ep', None, 'tp'), may hold values from -0.125 to 0.125
- expert_down: bfloat16 [16, 512, 2048], P('ep', 'tp'), may hold values from -0.25 to 0.25
- shared_gate: bfloat16 [2048, 512], P(None, 'tp'), may hold values from -0.125 to 0.125
- shared_up: bfloat16 [2048, 512], P(None, 'tp'), may hold values from -0.125 to 0.125
- shared_down: bfloat16 [512, 2048], P('tp'), may hold values from -0.25 to 0.25
Outputs:
- layer_out: bfloat16 [256, 2048], P('ep', 'tp')
- new_state: float32 [256, 8, 128, 128], P('ep', 'tp')
Inputs may be any that keep to these rules, and one draw needn't show every extreme that they name: `routes`: each token names 6 different experts. Among the tokens of one index of ep no expert is named by more than 16 tokens, and in every draw some expert is named by exactly 16 tokens of some index of ep.
All inputs are finite; a program needn't handle non-finite values.
Results may differ from a plain program's by a relative error of at most 0.017.
Values may be sent and summed in bfloat16 or wider, within the bound.
No kernel may reach another device: no remote copies, remote signals or barrier semaphores. Data moves between devices by JAX's collectives and lax.ppermute only.
A program may use at most 128 MiB of HBM per device.

v0:
```python
import jax
import jax.numpy as jnp
from jax import lax
from jax.sharding import PartitionSpec as P

epsilon = 1e-06
routed_scale = 2.5


def rms_scale(values, gain):
    return values * lax.rsqrt(jnp.mean(values * values, axis=-1, keepdims=True) + epsilon) * gain


def local(
    tokens,
    state,
    mix_gain,
    moe_gain,
    head_gain,
    w_forget,
    w_query,
    w_input,
    w_outgate,
    lower_bound,
    w_mix_out,
    routes,
    route_scores,
    expert_gate,
    expert_up,
    expert_down,
    shared_gate,
    shared_up,
    shared_down,
):
    seqs_here = tokens.shape[0]
    heads_here = state.shape[1]
    key_width = state.shape[2]
    value_width = state.shape[3]
    tokens_wide = tokens.astype(jnp.float32)
    normed = rms_scale(tokens_wide, mix_gain).astype(jnp.bfloat16)
    forget_pre = jnp.dot(normed, w_forget, preferred_element_type=jnp.float32).reshape(
        seqs_here, heads_here, key_width
    )
    query = jax.nn.silu(jnp.dot(normed, w_query, preferred_element_type=jnp.float32)).reshape(
        seqs_here, heads_here, key_width
    )
    input_val = jnp.dot(normed, w_input, preferred_element_type=jnp.float32).reshape(
        seqs_here, heads_here, value_width
    )
    gate_pre = jnp.dot(normed, w_outgate, preferred_element_type=jnp.float32).reshape(
        seqs_here, heads_here, value_width
    )
    bound_rows = lower_bound.reshape(heads_here, key_width)
    forget = bound_rows + (1.0 - bound_rows) * jax.nn.sigmoid(forget_pre)
    key_gate = (1.0 - bound_rows) * jax.nn.sigmoid(-forget_pre)
    new_state = forget[..., None] * state + key_gate[..., None] * input_val[:, :, None, :]
    readout = jnp.einsum("shkv,shk->shv", new_state, query, precision=lax.Precision.HIGHEST)
    gated_out = (rms_scale(readout, head_gain) * jax.nn.silu(gate_pre)).astype(jnp.bfloat16)
    gated_out = gated_out.reshape(seqs_here, heads_here * value_width)
    partial_value = jnp.dot(gated_out, w_mix_out, preferred_element_type=jnp.float32)
    mixer_out = lax.psum(partial_value.astype(jnp.bfloat16), "tp")
    residual = tokens_wide + mixer_out.astype(jnp.float32)
    moe_rows = rms_scale(residual, moe_gain).astype(jnp.bfloat16)
    full_width = moe_rows.shape[1]
    half_width = full_width // 2
    tp_index = lax.axis_index("tp")
    shared_hidden = (
        jax.nn.silu(jnp.dot(moe_rows, shared_gate, preferred_element_type=jnp.float32))
        * jnp.dot(moe_rows, shared_up, preferred_element_type=jnp.float32)
    ).astype(jnp.bfloat16)
    shared_part = jnp.dot(shared_hidden, shared_down, preferred_element_type=jnp.float32)
    shared_out = lax.psum_scatter(
        shared_part.astype(jnp.bfloat16), "tp", scatter_dimension=1, tiled=True
    )
    top_count = routes.shape[1]
    experts_all = expert_gate.shape[0] * lax.axis_size("ep")
    capacity = max(2, min(seqs_here, seqs_here * top_count * 3 // experts_all))
    flat_routes = routes.reshape(-1)
    onehot = (flat_routes[:, None] == jnp.arange(experts_all, dtype=jnp.int32)[None, :]).astype(
        jnp.int32
    )
    earlier = jnp.cumsum(onehot, axis=0) - onehot
    slot_rank = jnp.sum(earlier * onehot, axis=1)
    slot_index = flat_routes * capacity + slot_rank
    placing = (
        slot_index[None, :] == jnp.arange(experts_all * capacity, dtype=jnp.int32)[:, None]
    ).astype(jnp.int32)
    placing = (
        placing.reshape(experts_all * capacity, seqs_here, top_count)
        .sum(axis=2)
        .astype(jnp.bfloat16)
    )
    own_columns = lax.dynamic_slice_in_dim(moe_rows, tp_index * half_width, half_width, 1)
    outgoing = jnp.dot(placing, own_columns, preferred_element_type=jnp.float32).astype(
        jnp.bfloat16
    )
    outgoing = outgoing.reshape(experts_all, capacity, half_width)
    arrived_half = lax.all_to_all(outgoing, "ep", split_axis=0, concat_axis=1, tiled=True)
    arrived = lax.all_gather(arrived_half, "tp", axis=2, tiled=True)
    gate_act = jnp.einsum("esd,edf->esf", arrived, expert_gate, preferred_element_type=jnp.float32)
    up_act = jnp.einsum("esd,edf->esf", arrived, expert_up, preferred_element_type=jnp.float32)
    expert_hidden = (jax.nn.silu(gate_act) * up_act).astype(jnp.bfloat16)
    expert_part = jnp.einsum(
        "esf,efd->esd", expert_hidden, expert_down, preferred_element_type=jnp.float32
    )
    expert_half = lax.psum_scatter(
        expert_part.astype(jnp.bfloat16), "tp", scatter_dimension=2, tiled=True
    )
    returned = lax.all_to_all(expert_half, "ep", split_axis=1, concat_axis=0, tiled=True)
    pair_out = returned.reshape(experts_all * capacity, half_width)[slot_index].astype(jnp.float32)
    weights = route_scores / jnp.sum(route_scores, axis=-1, keepdims=True) * routed_scale
    routed = jnp.sum(
        pair_out.reshape(seqs_here, top_count, half_width) * weights[:, :, None], axis=1
    )
    residual_half = lax.dynamic_slice_in_dim(residual, tp_index * half_width, half_width, 1)
    layer_out = (residual_half + routed + shared_out.astype(jnp.float32)).astype(jnp.bfloat16)
    return (layer_out, new_state)


def solution(mesh):
    return jax.shard_map(
        local,
        mesh=mesh,
        in_specs=(
            P("ep", None),
            P("ep", "tp", None, None),
            P(),
            P(),
            P(),
            P(None, "tp"),
            P(None, "tp"),
            P(None, "tp"),
            P(None, "tp"),
            P("tp"),
            P("tp", None),
            P("ep", None),
            P("ep", None),
            P("ep", None, "tp"),
            P("ep", None, "tp"),
            P("ep", "tp", None),
            P(None, "tp"),
            P(None, "tp"),
            P("tp", None),
        ),
        out_specs=(P("ep", "tp"), P("ep", "tp", None, None)),
        check_vma=False,
    )
```

profile of v0, /device:TPU:0, one launch (start us, length us, event | category | flops | bytes accessed | tf_op | source)
XLA Modules:
  0.0 138.7 jit_solution(9879463072840509546)
XLA Ops:
  7.2 1.1 fusion.18
  8.4 2.1 %fusion.40 = f32[16,512]{1,0:T(8,128)S(1)} fusion(bf16[2048,512]{1,0:T(8,128)(2,1)} %param.27, bf16[16,2048]{1,0:T(8,128)(2,1)} %param.19, f32[2048]{0:T(1024)} %param.21, f32[16]{0:T(128)S(1)} %add_rsqrt_fusion.2), kind=kOutput, calls=%fused_computation.72 | convolution fusion | flops 33685504 | bytes 2203712 | tf_op jit(solution)/shard_map/dot_general | solution.py:50
  10.5 2.0 %fusion.44 = f32[16,512]{1,0:T(8,128)S(1)} fusion(bf16[2048,512]{1,0:T(8,128)(2,1)} %param.26, bf16[16,2048]{1,0:T(8,128)(2,1)S(1)} %copy-done.3, f32[2048]{0:T(1024)S(1)} %copy-done.5, f32[16]{0:T(128)S(1)} %add_rsqrt_fusion.2), kind=kOutput, calls=%fused_computation.74 | convolution fusion | flops 33685504 | bytes 2203712 | tf_op jit(solution)/shard_map/dot_general | solution.py:47
  12.5 2.0 %add_divide_fusion.1 = (f32[16,512]{1,0:T(8,128)S(1)}, f32[16,512]{1,0:T(8,128)S(1)}) fusion(bf16[2048,512]{1,0:T(8,128)(2,1)} %param.24, bf16[16,2048]{1,0:T(8,128)(2,1)S(1)} %copy-done.3, f32[2048]{0:T(1024)S(1)} %copy-done.5, f32[16]{0:T(128)S(1)} %add_rsqrt_fusion.2), kind=kOutput, calls=%fused_computation.46 | convolution fusion | flops 33726464 | bytes 2236480 | tf_op jit(solution)/shard_map/dot_general | solution.py:41
  14.6 2.0 %divide_multiply_fusion.1 = f32[16,512]{1,0:T(8,128)S(1)} fusion(bf16[2048,512]{1,0:T(8,128)(2,1)} %param.25, bf16[16,2048]{1,0:T(8,128)(2,1)S(1)} %copy-done.3, f32[2048]{0:T(1024)S(1)} %copy-done.5, f32[16]{0:T(128)S(1)} %add_rsqrt_fusion.2), kind=kOutput, calls=%fused_computation.43 | convolution fusion | flops 33718272 | bytes 2203712 | tf_op jit(solution)/shard_map/dot_general | solution.py:44
  16.7 4.4 %multiply_add_fusion = f32[16,4,128,128]{3,2,1,0:T(8,128)S(1)} fusion(f32[16,4,128,128]{3,2,1,0:T(8,128)} %param.20, f32[16,4,128]{2,1,0:T(4,128)S(1)} %mul.181, f32[16,4,128]{2,1,0:T(4,128)S(1)} %bitcast.70, f32[16,4,128]{2,1,0:T(4,128)S(1)} %bitcast.69), kind=kLoop, calls=%fused_computation.1 | loop fusion | flops 3145728 | bytes 8486912 | tf_op jit(solution)/shard_map/add | solution.py:56
  21.2 3.7 %fusion.50 = f32[16,4,1,128]{3,2,1,0:T(1,128)S(1)} fusion(f32[16,4,128,128]{3,2,1,0:T(8,128)S(1)} %multiply_add_fusion, f32[16,4,128,1]{2,3,1,0:T(1,128)S(1)} %bitcast.71), kind=kOutput, calls=%fused_computation.77 | convolution fusion | flops 12582912 | bytes 4259840 | tf_op jit(solution)/shard_map/shkv,shk->shv/dot_general | solution.py:57
  27.0 19.7 %all-reduce.2.cloned.1.call-done = bf16[16,2048]{1,0:T(8,128)(2,1)} async-done(((bf16[16,2048]{1,0:T(8,128)(2,1)}), bf16[16,2048]{1,0:T(8,128)(2,1)}) %all-reduce.2.cloned.1.call-update) | async-done | bytes 65552 | tf_op jit(solution)/shard_map/psum | solution.py:61
  46.8 1.6 %convert_add_fusion = (f32[16,2048]{1,0:T(8,128)}, f32[16]{0:T(128)S(1)}) fusion(bf16[16,2048]{1,0:T(8,128)(2,1)S(1)} %copy-done.3, bf16[16,2048]{1,0:T(8,128)(2,1)} %all-reduce.2.cloned.1.call-done), kind=kLoop, calls=%fused_computation.24 | loop fusion | flops 163824 | bytes 262208 | tf_op jit(solution)/shard_map/add | solution.py:62
  49.6 22.2 %all_to_all.21 = bf16[16,16,1024]{2,1,0:T(8,128)(2,1)} all-to-all(bf16[16,16,1024]{2,1,0:T(8,128)(2,1)S(1)} %bitcast.66), channel_id=1, replica_groups=mesh['ep'=16,'tp'=2] {'ep'}, dimensions={0} | all-to-all | bytes 1048576 | tf_op jit(solution)/shard_map/all_to_all | solution.py:98
  72.1 7.3 %all-gather.2.cloned.1.call-done = bf16[1,256,2048]{2,1,0:T(8,128)(2,1)} async-done(((bf16[1,256,1024]{2,1,0:T(8,128)(2,1)}), bf16[1,256,2048]{2,1,0:T(8,128)(2,1)}) %all-gather.2.cloned.1.call-update) | async-done | bytes 1048592 | tf_op jit(solution)/shard_map/all_gather | solution.py:99
  79.4 2.1 %fusion.5 = f32[256,256]{1,0:T(8,128)S(1)} fusion(bf16[1,2048,256]{2,1,0:T(8,128)(2,1)} %param.32, bf16[1,256,2048]{2,1,0:T(8,128)(2,1)} %all-gather.2.cloned.1.call-done), kind=kOutput, calls=%fused_computation.13 | convolution fusion | flops 268435456 | bytes 2359296 | tf_op jit(solution)/shard_map/esd,edf->esf/dot_general | solution.py:100
  81.5 3.8 %fusion = bf16[1,256,2048]{2,1,0:T(8,128)(2,1)} fusion(bf16[1,256,2048]{2,1,0:T(8,128)(2,1)} %param.34, bf16[1,2048,256]{2,1,0:T(8,128)(2,1)} %param.33, bf16[1,256,2048]{2,1,0:T(8,128)(2,1)S(1)} %copy-done.2, f32[256,256]{1,0:T(8,128)S(1)} %fusion.5), kind=kOutput, calls=%fused_computation.3 | convolution fusion | flops 537788416 | bytes 4456448 | tf_op jit(solution)/shard_map/esf,efd->esd/dot_general | solution.py:103
  85.5 9.6 %reduce-scatter.3.cloned.1.call-done = bf16[1,256,1024]{2,1,0:T(8,128)(2,1)} async-done(((bf16[1,256,2048]{2,1,0:T(8,128)(2,1)}), bf16[1,256,1024]{2,1,0:T(8,128)(2,1)}) %reduce-scatter.3.cloned.1.call-update) | async-done | bytes 524304 | tf_op jit(solution)/shard_map/reduce_scatter | solution.py:106
  95.1 1.9 %copy.51 = bf16[1,256,1024]{2,0,1:T(2,128)(2,1)S(1)} copy(bf16[1,256,1024]{2,1,0:T(8,128)(2,1)} %reduce-scatter.3.cloned.1.call-done) | data formatting | bytes 1048576 | tf_op jit(solution)/shard_map/reduce_scatter | solution.py:106
  97.4 4.5 %reduce = bf16[256,1024]{1,0:T(8,128)(2,1)} reduce(bf16[256,1,1024]{2,1,0:T(2,128)(2,1)S(1)} %bitcast.64, bf16[]{:T(256)} %broadcast.158), dimensions={1}, to_apply=%bitcast.55.reduce_sub_computation | reduce | bytes 1048578
  101.9 2.2 %reshape.191 = bf16[16,2,8192]{2,1,0:T(2,128)(2,1)} reshape(bf16[256,1024]{1,0:T(8,128)(2,1)} %reduce) | data formatting | bytes 1048576
  104.1 6.8 %all-to-all-start.1 = ((bf16[16,2,8192]{2,1,0:T(2,128)(2,1)}), bf16[16,2,8192]{2,1,0:T(2,128)(2,1)S(1)}, u32[]{:S(2)}, u32[]{:S(2)}) async-start(bf16[16,2,8192]{2,1,0:T(2,128)(2,1)} %reshape.191), calls=%async_computation.2 | async-start | bytes 1048576 | tf_op jit(solution)/shard_map/all_to_all | solution.py:109
  111.1 1.5 %fusion.51 = f32[16,256]{1,0:T(8,128)S(1)} fusion(bf16[16,2048]{1,0:T(8,128)(2,1)S(1)} %multiply_convert_fusion, bf16[2048,256]{1,0:T(8,128)(2,1)} %param.35), kind=kOutput, calls=%fused_computation.78 | convolution fusion | flops 16777216 | bytes 1130496 | tf_op jit(solution)/shard_map/dot_general | solution.py:68
  112.6 2.9 %convolution_convert_fusion.1 = bf16[16,2048]{1,0:T(8,128)(2,1)} fusion(bf16[256,2048]{1,0:T(8,128)(2,1)} %param.37, bf16[16,2048]{1,0:T(8,128)(2,1)S(1)} %multiply_convert_fusion, bf16[2048,256]{1,0:T(8,128)(2,1)} %param.36, f32[16,256]{1,0:T(8,128)S(1)} %fusion.51), kind=kOutput, calls=%fused_computation.4 | convolution fusion | flops 33611776 | bytes 2244608 | tf_op jit(solution)/shard_map/dot_general | solution.py:71
  115.5 10.9 %all-to-all-done.1 = bf16[16,2,8192]{2,1,0:T(2,128)(2,1)S(1)} async-done(((bf16[16,2,8192]{2,1,0:T(2,128)(2,1)}), bf16[16,2,8192]{2,1,0:T(2,128)(2,1)S(1)}, u32[]{:S(2)}, u32[]{:S(2)}) %all-to-all-start.1) | async-done | bytes 524320 | tf_op jit(solution)/shard_map/all_to_all | solution.py:109
  126.4 1.8 %reshape.192 = bf16[256,1,1024]{2,1,0:T(2,128)(2,1)} reshape(bf16[16,2,8192]{2,1,0:T(2,128)(2,1)S(1)} %all-to-all-done.1) | data formatting | bytes 1048576
  128.2 1.4 %copy.50 = bf16[1,256,1024]{2,1,0:T(8,128)(2,1)S(1)} copy(bf16[1,256,1024]{2,0,1:T(2,128)(2,1)} %bitcast.63) | data formatting | bytes 1048576
  130.8 1.4 %add_convert_fusion = bf16[16,1024]{1,0:T(8,128)(2,1)} fusion(bf16[16,1024]{1,0:T(8,128)(2,1)} %reduce-scatter.5.cloned.1.call-done, f32[16,1024]{1,0:T(8,128)S(1)} %multiply_reduce_fusion, f32[16,2048]{1,0:T(8,128)S(1)} %copy-done.4, s32[]{:T(128)S(6)} %select_n.14), kind=kLoop, calls=%fused_computation.35 | loop fusion | flops 65536 | bytes 196612 | tf_op jit(solution)/shard_map/convert_element_type | solution.py:116
  (67 shorter events, 5.7 us)
Async XLA Ops:
  7.2 17.9 %copy-start = (bf16[512,2048]{1,0:T(8,128)(2,1)S(1)}, bf16[512,2048]{1,0:T(8,128)(2,1)}, u32[]{:S(2)}) copy-start(bf16[512,2048]{1,0:T(8,128)(2,1)} %param.29) | copy-start | bytes 6291460
  7.2 3.3 %copy-start.3 = (bf16[16,2048]{1,0:T(8,128)(2,1)S(1)}, bf16[16,2048]{1,0:T(8,128)(2,1)}, u32[]{:S(2)}) copy-start(bf16[16,2048]{1,0:T(8,128)(2,1)} %param.19) | copy-start | bytes 196612
  7.2 3.3 %copy-start.5 = (f32[2048]{0:T(1024)S(1)}, f32[2048]{0:T(1024)}, u32[]{:S(2)}) copy-start(f32[2048]{0:T(1024)} %param.21) | copy-start | bytes 24580
  7.2 39.6 %all-reduce.2.cloned.1.call-start = ((), (), s32[]{:S(2)}) async-start(), calls=%async_computation.4 | async-start | bytes 131072 | tf_op jit(solution)/shard_map/psum | solution.py:61
  10.5 4.1 %copy-start.8 = (f32[512]{0:T(512)S(1)}, f32[512]{0:T(512)}, u32[]{:S(2)}) copy-start(f32[512]{0:T(512)} %param.28) | copy-start | bytes 6148
  21.1 3.7 %copy-start.1 = (f32[16,4,128,128]{3,2,1,0:T(8,128)}, f32[16,4,128,128]{3,2,1,0:T(8,128)S(1)}, u32[]{:S(2)}) copy-start(f32[16,4,128,128]{3,2,1,0:T(8,128)S(1)} %multiply_add_fusion) | copy-start | bytes 12582916
  21.2 3.8 %copy-start.10 = (f32[128]{0:T(128)S(1)}, f32[128]{0:T(128)}, u32[]{:S(2)}) copy-start(f32[128]{0:T(128)} %param.23) | copy-start | bytes 1540
  24.8 1.3 copy-start.9
  24.8 23.5 %copy-start.7 = (f32[2048]{0:T(1024)S(1)}, f32[2048]{0:T(1024)}, u32[]{:S(2)}) copy-start(f32[2048]{0:T(1024)} %param.22) | copy-start | bytes 24580
  26.1 53.3 %all-gather.2.cloned.1.call-start = ((), (), s32[]{:S(2)}) async-start(), calls=%async_computation.5 | async-start | bytes 1572864 | tf_op jit(solution)/shard_map/all_gather | solution.py:99
  71.9 23.2 %reduce-scatter.3.cloned.1.call-start = ((), (), s32[]{:S(2)}) async-start(), calls=%async_computation.6 | async-start | bytes 1572864 | tf_op jit(solution)/shard_map/reduce_scatter | solution.py:106
  79.4 2.1 %copy-start.2 = (bf16[1,256,2048]{2,1,0:T(8,128)(2,1)S(1)}, bf16[1,256,2048]{2,1,0:T(8,128)(2,1)}, u32[]{:S(2)}) copy-start(bf16[1,256,2048]{2,1,0:T(8,128)(2,1)} %all-gather.2.cloned.1.call-done) | copy-start | bytes 3145732
  81.5 3.9 %copy-start.6 = (f32[16,6]{0,1:T(8,128)S(1)}, f32[16,6]{0,1:T(8,128)}, u32[]{:S(2)}) copy-start(f32[16,6]{0,1:T(8,128)} %param.31) | copy-start | bytes 1156
  104.1 22.3 %all-to-all-start.1 = ((bf16[16,2,8192]{2,1,0:T(2,128)(2,1)}), bf16[16,2,8192]{2,1,0:T(2,128)(2,1)S(1)}, u32[]{:S(2)}, u32[]{:S(2)}) async-start(bf16[16,2,8192]{2,1,0:T(2,128)(2,1)} %reshape.191), calls=%async_computation.2 | async-start | bytes 1048576 | tf_op jit(solution)/shard_map/all_to_all | solution.py:109
  110.9 19.8 %reduce-scatter.5.cloned.1.call-start = ((), (), s32[]{:S(2)}) async-start(), calls=%async_computation.7 | async-start | bytes 98304 | tf_op jit(solution)/shard_map/reduce_scatter | solution.py:72
  128.2 2.5 %copy-start.4 = (f32[16,2048]{1,0:T(8,128)S(1)}, f32[16,2048]{1,0:T(8,128)}, u32[]{:S(2)}) copy-start(f32[16,2048]{1,0:T(8,128)} %get-tuple-element.2) | copy-start | bytes 393220
Sparse Core Ops, SparseCore 0:
  26.2 20.4 all-reduce.1
  72.0 7.3 all-gather.1
  85.5 9.5 reduce-scatter.2
  115.6 8.8 reduce-scatter.4
where the time goes:
time: 140 us; the launch traced here: 139 us
  waiting for transfers between devices  47.6 us (34%)
  matrix products  23.4 us (17%)
  blocking collectives  22.2 us (16%)
  other arithmetic  14.9 us (11%)
  between operations  14.1 us (10%)
  local copies, waits for them, and re-layouts  9.27 us (7%)
  starting transfers between devices  7.14 us (5%)
    all_to_all x1, blocking collectives, local(): lax.all_to_all(outgoing, 'ep', split_axis=0, concat_axis=1, tiled=True)  22.2 us
    psum x1, waiting for transfers between devices, local(): mixer_out = lax.psum(partial_value.astype(jnp.bfloat16), 'tp')  19.7 us
    all_to_all x1, waiting for transfers between devices, local(): lax.all_to_all(expert_half, 'ep', split_axis=1, concat_axis=0, tiled=True)  10.9 us
    reduce_scatter x1, waiting for transfers between devices, local(): lax.psum_scatter(expert_part.astype(jnp.bfloat16), 'tp', scatter_dimensio...  9.58 us
    all_gather x1, waiting for transfers between devices, local(): arrived = lax.all_gather(arrived_half, 'tp', axis=2, tiled=True)  7.3 us
    all_to_all x1, starting transfers between devices, local(): lax.all_to_all(expert_half, 'ep', split_axis=1, concat_axis=0, tiled=True)  6.79 us
    unnamed x29, local copies, waits for them, and re-layouts  6.09 us
    unnamed x1, other arithmetic  4.5 us
  transfers between devices with their start and end apart: 5, of which 4 were waited for; matrix products, arithmetic and copies ran while one was open for 7% of the time, Pallas kernels for 0%

commit v1 on v0

--- a/solution.py
+++ b/solution.py
@@ -2,6 +2,7 @@
 import jax.numpy as jnp
 from jax import lax
 from jax.sharding import PartitionSpec as P
+from jax.lax import all_gather
 
 epsilon = 1e-06
 routed_scale = 2.5
@@ -58,7 +59,8 @@
     gated_out = (rms_scale(readout, head_gain) * jax.nn.silu(gate_pre)).astype(jnp.bfloat16)
     gated_out = gated_out.reshape(seqs_here, heads_here * value_width)
     partial_value = jnp.dot(gated_out, w_mix_out, preferred_element_type=jnp.float32)
-    mixer_out = lax.psum(partial_value.astype(jnp.bfloat16), "tp")
+    inputs = partial_value.astype(jnp.bfloat16)
+    mixer_out = jnp.sum(all_gather(inputs, "tp"), axis=0)
     residual = tokens_wide + mixer_out.astype(jnp.float32)
     moe_rows = rms_scale(residual, moe_gain).astype(jnp.bfloat16)
     full_width = moe_rows.shape[1]

time: 140 us -> 121 us (0.86)
  waiting for transfers between devices: 47.6 us -> 27.8 us
  blocking collectives: 22.2 us -> 25.5 us
  other arithmetic: 14.9 us -> 13.3 us
    psum x1 -> x0, waiting for transfers between devices: 19.7 us -> none  [local(): mixer_out = lax.psum(partial_value.astype(jnp.bfloat16), 'tp')]
    all_gather x0 -> x1, blocking collectives: none -> 2.03 us  [local(): mixer_out = jnp.sum(all_gather(inputs, 'tp'), axis=0)]
  transfers between devices with their start and end apart: 5 -> 4, of which waited for: 4 -> 3; matrix products, arithmetic and copies ran while one was open for 7% -> 7% of each run, Pallas kernels for 0% -> 0%
where the time goes in v1:
time: 121 us; the launch traced here: 120 us
  waiting for transfers between devices  27.8 us (23%)
  blocking collectives  25.5 us (21%)
  matrix products  22.8 us (19%)
  between operations  14.1 us (12%)
  other arithmetic  13.3 us (11%)
  local copies, waits for them, and re-layouts  9.27 us (8%)
  starting transfers between devices  7.23 us (6%)
    all_to_all x1, blocking collectives, local(): lax.all_to_all(outgoing, 'ep', split_axis=0, concat_axis=1, tiled=True)  23.5 us
    all_to_all x1, waiting for transfers between devices, local(): lax.all_to_all(expert_half, 'ep', split_axis=1, concat_axis=0, tiled=True)  10.8 us
    reduce_scatter x1, waiting for transfers between devices, local(): lax.psum_scatter(expert_part.astype(jnp.bfloat16), 'tp', scatter_dimensio...  9.7 us
    all_gather x1, waiting for transfers between devices, local(): arrived = lax.all_gather(arrived_half, 'tp', axis=2, tiled=True)  7.28 us
    all_to_all x1, starting transfers between devices, local(): lax.all_to_all(expert_half, 'ep', split_axis=1, concat_axis=0, tiled=True)  6.92 us
    unnamed x29, local copies, waits for them, and re-layouts  6.09 us
    unnamed x1, other arithmetic  4.5 us
    add x1, other arithmetic, local(): forget[..., None] * state + key_gate[..., None] * input_val[:, :, None, :]  4.39 us
  transfers between devices with their start and end apart: 4, of which 3 were waited for; matrix products, arithmetic and copies ran while one was open for 7% of the time, Pallas kernels for 0%

profile of v1, /device:TPU:0, one launch (start us, length us, event | category | flops | bytes accessed | tf_op | source)
XLA Modules:
  0.0 120.0 jit_solution(10027260449461363775)
XLA Ops:
  7.3 1.1 fusion.18
  8.4 2.1 %fusion.40 = f32[16,512]{1,0:T(8,128)S(1)} fusion(bf16[2048,512]{1,0:T(8,128)(2,1)} %param.27, bf16[16,2048]{1,0:T(8,128)(2,1)} %param.19, f32[2048]{0:T(1024)} %param.21, f32[16]{0:T(128)S(1)} %add_rsqrt_fusion.2), kind=kOutput, calls=%fused_computation.72 | convolution fusion | flops 33685504 | bytes 2203712 | tf_op jit(solution)/shard_map/dot_general | solution.py:51
  10.5 2.0 %fusion.44 = f32[16,512]{1,0:T(8,128)S(1)} fusion(bf16[2048,512]{1,0:T(8,128)(2,1)} %param.26, bf16[16,2048]{1,0:T(8,128)(2,1)S(1)} %copy-done.3, f32[2048]{0:T(1024)S(1)} %copy-done.5, f32[16]{0:T(128)S(1)} %add_rsqrt_fusion.2), kind=kOutput, calls=%fused_computation.74 | convolution fusion | flops 33685504 | bytes 2203712 | tf_op jit(solution)/shard_map/dot_general | solution.py:48
  12.5 2.0 %add_divide_fusion.1 = (f32[16,512]{1,0:T(8,128)S(1)}, f32[16,512]{1,0:T(8,128)S(1)}) fusion(bf16[2048,512]{1,0:T(8,128)(2,1)} %param.24, bf16[16,2048]{1,0:T(8,128)(2,1)S(1)} %copy-done.3, f32[2048]{0:T(1024)S(1)} %copy-done.5, f32[16]{0:T(128)S(1)} %add_rsqrt_fusion.2), kind=kOutput, calls=%fused_computation.46 | convolution fusion | flops 33726464 | bytes 2236480 | tf_op jit(solution)/shard_map/dot_general | solution.py:42
  14.6 2.0 %divide_multiply_fusion.1 = f32[16,512]{1,0:T(8,128)S(1)} fusion(bf16[2048,512]{1,0:T(8,128)(2,1)} %param.25, bf16[16,2048]{1,0:T(8,128)(2,1)S(1)} %copy-done.3, f32[2048]{0:T(1024)S(1)} %copy-done.5, f32[16]{0:T(128)S(1)} %add_rsqrt_fusion.2), kind=kOutput, calls=%fused_computation.43 | convolution fusion | flops 33718272 | bytes 2203712 | tf_op jit(solution)/shard_map/dot_general | solution.py:45
  16.7 4.4 %multiply_add_fusion = f32[16,4,128,128]{3,2,1,0:T(8,128)S(1)} fusion(f32[16,4,128,128]{3,2,1,0:T(8,128)} %param.20, f32[16,4,128]{2,1,0:T(4,128)S(1)} %mul.181, f32[16,4,128]{2,1,0:T(4,128)S(1)} %bitcast.72, f32[16,4,128]{2,1,0:T(4,128)S(1)} %bitcast.71), kind=kLoop, calls=%fused_computation.1 | loop fusion | flops 3145728 | bytes 8486912 | tf_op jit(solution)/shard_map/add | solution.py:57
  21.2 3.7 %fusion.50 = f32[16,4,1,128]{3,2,1,0:T(1,128)S(1)} fusion(f32[16,4,128,128]{3,2,1,0:T(8,128)S(1)} %multiply_add_fusion, f32[16,4,128,1]{2,3,1,0:T(1,128)S(1)} %bitcast.73), kind=kOutput, calls=%fused_computation.77 | convolution fusion | flops 12582912 | bytes 4259840 | tf_op jit(solution)/shard_map/shkv,shk->shv/dot_general | solution.py:58
  25.5 2.0 %all-gather = bf16[32,2048]{1,0:T(8,128)(2,1)S(1)} all-gather(bf16[16,2048]{1,0:T(8,128)(2,1)S(1)} %convolution_convert_fusion.2), channel_id=2, replica_groups=mesh['ep'=16,'tp'=2] {'tp'}, dimensions={0}, use_global_device_ids=true | all-gather | bytes 196608 | tf_op jit(solution)/shard_map/all_gather | solution.py:63
  29.6 23.5 %all_to_all.21 = bf16[16,16,1024]{2,1,0:T(8,128)(2,1)} all-to-all(bf16[16,16,1024]{2,1,0:T(8,128)(2,1)S(1)} %bitcast.67), channel_id=1, replica_groups=mesh['ep'=16,'tp'=2] {'ep'}, dimensions={0} | all-to-all | bytes 1048576 | tf_op jit(solution)/shard_map/all_to_all | solution.py:100
  53.4 7.3 %all-gather.3.cloned.1.call-done = bf16[1,256,2048]{2,1,0:T(8,128)(2,1)} async-done(((bf16[1,256,1024]{2,1,0:T(8,128)(2,1)}), bf16[1,256,2048]{2,1,0:T(8,128)(2,1)}) %all-gather.3.cloned.1.call-update) | async-done | bytes 1048592 | tf_op jit(solution)/shard_map/all_gather | solution.py:101
  60.6 2.1 %fusion.5 = f32[256,256]{1,0:T(8,128)S(1)} fusion(bf16[1,2048,256]{2,1,0:T(8,128)(2,1)} %param.32, bf16[1,256,2048]{2,1,0:T(8,128)(2,1)} %all-gather.3.cloned.1.call-done), kind=kOutput, calls=%fused_computation.13 | convolution fusion | flops 268435456 | bytes 2359296 | tf_op jit(solution)/shard_map/esd,edf->esf/dot_general | solution.py:102
  62.7 3.8 %fusion = bf16[1,256,2048]{2,1,0:T(8,128)(2,1)} fusion(bf16[1,256,2048]{2,1,0:T(8,128)(2,1)} %param.34, bf16[1,2048,256]{2,1,0:T(8,128)(2,1)} %param.33, bf16[1,256,2048]{2,1,0:T(8,128)(2,1)S(1)} %copy-done.2, f32[256,256]{1,0:T(8,128)S(1)} %fusion.5), kind=kOutput, calls=%fused_computation.3 | convolution fusion | flops 537788416 | bytes 4456448 | tf_op jit(solution)/shard_map/esf,efd->esd/dot_general | solution.py:105
  66.6 9.7 %reduce-scatter.3.cloned.1.call-done = bf16[1,256,1024]{2,1,0:T(8,128)(2,1)} async-done(((bf16[1,256,2048]{2,1,0:T(8,128)(2,1)}), bf16[1,256,1024]{2,1,0:T(8,128)(2,1)}) %reduce-scatter.3.cloned.1.call-update) | async-done | bytes 524304 | tf_op jit(solution)/shard_map/reduce_scatter | solution.py:108
  76.3 1.9 %copy.51 = bf16[1,256,1024]{2,0,1:T(2,128)(2,1)S(1)} copy(bf16[1,256,1024]{2,1,0:T(8,128)(2,1)} %reduce-scatter.3.cloned.1.call-done) | data formatting | bytes 1048576 | tf_op jit(solution)/shard_map/reduce_scatter | solution.py:108
  78.6 4.5 %reduce.1 = bf16[256,1024]{1,0:T(8,128)(2,1)} reduce(bf16[256,1,1024]{2,1,0:T(2,128)(2,1)S(1)} %bitcast.65, bf16[]{:T(256)} %broadcast.158), dimensions={1}, to_apply=%bitcast.56.reduce_sub_computation | reduce | bytes 1048578
  83.1 2.2 %reshape.192 = bf16[16,2,8192]{2,1,0:T(2,128)(2,1)} reshape(bf16[256,1024]{1,0:T(8,128)(2,1)} %reduce.1) | data formatting | bytes 1048576
  85.4 6.9 %all-to-all-start.1 = ((bf16[16,2,8192]{2,1,0:T(2,128)(2,1)}), bf16[16,2,8192]{2,1,0:T(2,128)(2,1)S(1)}, u32[]{:S(2)}, u32[]{:S(2)}) async-start(bf16[16,2,8192]{2,1,0:T(2,128)(2,1)} %reshape.192), calls=%async_computation.2 | async-start | bytes 1048576 | tf_op jit(solution)/shard_map/all_to_all | solution.py:111
  92.3 1.5 %fusion.51 = f32[16,256]{1,0:T(8,128)S(1)} fusion(bf16[16,2048]{1,0:T(8,128)(2,1)S(1)} %multiply_convert_fusion, bf16[2048,256]{1,0:T(8,128)(2,1)} %param.35), kind=kOutput, calls=%fused_computation.78 | convolution fusion | flops 16777216 | bytes 1130496 | tf_op jit(solution)/shard_map/dot_general | solution.py:70
  93.8 2.9 %convolution_convert_fusion.1 = bf16[16,2048]{1,0:T(8,128)(2,1)} fusion(bf16[256,2048]{1,0:T(8,128)(2,1)} %param.37, bf16[16,2048]{1,0:T(8,128)(2,1)S(1)} %multiply_convert_fusion, bf16[2048,256]{1,0:T(8,128)(2,1)} %param.36, f32[16,256]{1,0:T(8,128)S(1)} %fusion.51), kind=kOutput, calls=%fused_computation.4 | convolution fusion | flops 33611776 | bytes 2244608 | tf_op jit(solution)/shard_map/dot_general | solution.py:73
  97.0 10.8 %all-to-all-done.1 = bf16[16,2,8192]{2,1,0:T(2,128)(2,1)S(1)} async-done(((bf16[16,2,8192]{2,1,0:T(2,128)(2,1)}), bf16[16,2,8192]{2,1,0:T(2,128)(2,1)S(1)}, u32[]{:S(2)}, u32[]{:S(2)}) %all-to-all-start.1) | async-done | bytes 524320 | tf_op jit(solution)/shard_map/all_to_all | solution.py:111
  107.8 1.8 %reshape.193 = bf16[256,1,1024]{2,1,0:T(2,128)(2,1)} reshape(bf16[16,2,8192]{2,1,0:T(2,128)(2,1)S(1)} %all-to-all-done.1) | data formatting | bytes 1048576
  109.6 1.4 %copy.50 = bf16[1,256,1024]{2,1,0:T(8,128)(2,1)S(1)} copy(bf16[1,256,1024]{2,0,1:T(2,128)(2,1)} %bitcast.64) | data formatting | bytes 1048576
  111.0 0.8 gather_fusion
  112.1 1.4 %add_convert_fusion = bf16[16,1024]{1,0:T(8,128)(2,1)} fusion(bf16[16,1024]{1,0:T(8,128)(2,1)} %reduce-scatter.5.cloned.1.call-done, f32[16,1024]{1,0:T(8,128)S(1)} %multiply_reduce_fusion, f32[16,2048]{1,0:T(8,128)S(1)} %copy-done.4, s32[]{:T(128)S(6)} %select_n.14), kind=kLoop, calls=%fused_computation.35 | loop fusion | flops 65536 | bytes 196612 | tf_op jit(solution)/shard_map/convert_element_type | solution.py:118
  (66 shorter events, 4.2 us)
Async XLA Ops:
  7.2 17.9 %copy-start = (bf16[512,2048]{1,0:T(8,128)(2,1)S(1)}, bf16[512,2048]{1,0:T(8,128)(2,1)}, u32[]{:S(2)}) copy-start(bf16[512,2048]{1,0:T(8,128)(2,1)} %param.29) | copy-start | bytes 6291460
  7.2 3.3 %copy-start.3 = (bf16[16,2048]{1,0:T(8,128)(2,1)S(1)}, bf16[16,2048]{1,0:T(8,128)(2,1)}, u32[]{:S(2)}) copy-start(bf16[16,2048]{1,0:T(8,128)(2,1)} %param.19) | copy-start | bytes 196612
  7.2 3.3 %copy-start.5 = (f32[2048]{0:T(1024)S(1)}, f32[2048]{0:T(1024)}, u32[]{:S(2)}) copy-start(f32[2048]{0:T(1024)} %param.21) | copy-start | bytes 24580
  7.2 53.4 %all-gather.3.cloned.1.call-start = ((), (), s32[]{:S(2)}) async-start(), calls=%async_computation.4 | async-start | bytes 1572864 | tf_op jit(solution)/shard_map/all_gather | solution.py:101
  10.5 4.1 %copy-start.8 = (f32[512]{0:T(512)S(1)}, f32[512]{0:T(512)}, u32[]{:S(2)}) copy-start(f32[512]{0:T(512)} %param.28) | copy-start | bytes 6148
  21.1 3.7 %copy-start.1 = (f32[16,4,128,128]{3,2,1,0:T(8,128)}, f32[16,4,128,128]{3,2,1,0:T(8,128)S(1)}, u32[]{:S(2)}) copy-start(f32[16,4,128,128]{3,2,1,0:T(8,128)S(1)} %multiply_add_fusion) | copy-start | bytes 12582916
  21.2 3.8 %copy-start.10 = (f32[128]{0:T(128)S(1)}, f32[128]{0:T(128)}, u32[]{:S(2)}) copy-start(f32[128]{0:T(128)} %param.23) | copy-start | bytes 1540
  24.8 3.5 %copy-start.9 = (s32[16,6]{0,1:T(8,128)S(1)}, s32[16,6]{0,1:T(8,128)}, u32[]{:S(2)}) copy-start(s32[16,6]{0,1:T(8,128)} %param.30) | copy-start | bytes 1156
  24.8 4.3 %copy-start.7 = (f32[2048]{0:T(1024)S(1)}, f32[2048]{0:T(1024)}, u32[]{:S(2)}) copy-start(f32[2048]{0:T(1024)} %param.22) | copy-start | bytes 24580
  53.1 23.1 %reduce-scatter.3.cloned.1.call-start = ((), (), s32[]{:S(2)}) async-start(), calls=%async_computation.5 | async-start | bytes 1572864 | tf_op jit(solution)/shard_map/reduce_scatter | solution.py:108
  60.6 2.1 %copy-start.2 = (bf16[1,256,2048]{2,1,0:T(8,128)(2,1)S(1)}, bf16[1,256,2048]{2,1,0:T(8,128)(2,1)}, u32[]{:S(2)}) copy-start(bf16[1,256,2048]{2,1,0:T(8,128)(2,1)} %all-gather.3.cloned.1.call-done) | copy-start | bytes 3145732
  85.4 11.5 %copy-start.6 = (f32[16,6]{0,1:T(8,128)S(1)}, f32[16,6]{0,1:T(8,128)}, u32[]{:S(2)}) copy-start(f32[16,6]{0,1:T(8,128)} %param.31) | copy-start | bytes 1156
  85.4 22.4 %all-to-all-start.1 = ((bf16[16,2,8192]{2,1,0:T(2,128)(2,1)}), bf16[16,2,8192]{2,1,0:T(2,128)(2,1)S(1)}, u32[]{:S(2)}, u32[]{:S(2)}) async-start(bf16[16,2,8192]{2,1,0:T(2,128)(2,1)} %reshape.192), calls=%async_computation.2 | async-start | bytes 1048576 | tf_op jit(solution)/shard_map/all_to_all | solution.py:111
  92.3 19.8 %reduce-scatter.5.cloned.1.call-start = ((), (), s32[]{:S(2)}) async-start(), calls=%async_computation.6 | async-start | bytes 98304 | tf_op jit(solution)/shard_map/reduce_scatter | solution.py:74
  109.6 2.5 %copy-start.4 = (f32[16,2048]{1,0:T(8,128)S(1)}, f32[16,2048]{1,0:T(8,128)}, u32[]{:S(2)}) copy-start(f32[16,2048]{1,0:T(8,128)} %get-tuple-element.2) | copy-start | bytes 393220
Sparse Core Ops, SparseCore 0:
  53.2 7.3 all-gather.2
  66.7 9.5 reduce-scatter.2
  96.9 8.8 reduce-scatter.4
